TPU v7x, 32 devices: a whole 2x2x4 slice. The times are simulated.
32 devices in a mesh: rep: 2 (over x), fs: 8 (over z, y), tp: 2 (over core).
Axes of the slice: x: 2, y: 2, z: 4, core: 2. Of those that a mesh axis runs over, the one named last changes fastest.
Arguments:
- tokens: bfloat16 [8192, 2048], P(('rep', 'fs')), may hold values from -6 to 6
- mix_gain: bfloat16 [2048], replicated, may hold values from 0.099609375 to 1.8984375
- value_weight: bfloat16 [2048, 1536], P('fs', 'tp'), may hold values from -0.125 to 0.125
- outer_gate_weight: bfloat16 [2048, 1536], P('fs', 'tp'), may hold values from -0.125 to 0.125
- inner_gate_weight: bfloat16 [2048, 1536], P('fs', 'tp'), may hold values from -0.125 to 0.125
- conv_taps: bfloat16 [3, 1536], P(None, 'tp'), may hold values from -3 to 3
- mix_out_weight: bfloat16 [1536, 2048], P('tp', 'fs'), may hold values from -0.15625 to 0.15625
- ffn_gain: bfloat16 [2048], replicated, may hold values from 0.099609375 to 1.8984375
- gate_weight: bfloat16 [2048, 4096], P('fs', 'tp'), may hold values from -0.125 to 0.125
- up_weight: bfloat16 [2048, 4096], P('fs', 'tp'), may hold values from -0.125 to 0.125
- down_weight: bfloat16 [4096, 2048], P('tp', 'fs'), may hold values from -0.09375 to 0.09375
Outputs:
- layer_out: bfloat16 [8192, 2048], P(('rep', 'fs'))
All inputs are finite; a program needn't handle non-finite values.
Results may differ from a plain program's by a relative error of at most 0.02.
Values may be sent and summed in bfloat16 or wider, within the bound.
A program may use at most 128 MiB of HBM per device.

v0:
```python
import jax
import jax.numpy as jnp
from jax import lax
from jax.sharding import PartitionSpec as P

SEQ_GRP = 2
EPS = 1e-05


def rms_norm(values, gain):
    floats = values.astype(jnp.float32)
    scaled = floats * lax.rsqrt(jnp.mean(floats * floats, axis=-1, keepdims=True) + EPS)
    return (scaled * gain.astype(jnp.float32)).astype(jnp.bfloat16)


def short_conv(value_proj, outer_proj, inner_proj, conv_taps, seq_len):
    mixed_in = inner_proj.astype(jnp.float32) * value_proj.astype(jnp.float32)
    count_rows = mixed_in.shape[0]
    position = (jnp.arange(count_rows, dtype=jnp.int32) % seq_len)[:, None]
    zero_row = jnp.zeros((1, mixed_in.shape[1]), jnp.float32)
    back_one = jnp.where(position >= 1, jnp.concatenate([zero_row, mixed_in[:-1]], axis=0), 0.0)
    back_two = jnp.where(
        position >= 2, jnp.concatenate([zero_row, zero_row, mixed_in[:-2]], axis=0), 0.0
    )
    taps = conv_taps.astype(jnp.float32)
    convolved = taps[0] * back_two + taps[1] * back_one + taps[2] * mixed_in
    return (outer_proj.astype(jnp.float32) * convolved).astype(jnp.bfloat16)


def shifted(values, axis, step):
    size = lax.axis_size(axis)
    return lax.ppermute(values, axis, [(i, (i + step) % size) for i in range(size)])


def spread(block, axis):
    size, me, rows = (lax.axis_size(axis), lax.axis_index(axis), block.shape[0])
    if size == 2:
        other = shifted(block, axis, 1)
        first = me == 0
        return jnp.concatenate([jnp.where(first, block, other), jnp.where(first, other, block)])
    whole = jnp.zeros((size * rows,) + block.shape[1:], block.dtype)
    for step in range(size):
        piece = block if step == 0 else shifted(block, axis, step)
        whole = lax.dynamic_update_slice_in_dim(whole, piece, (me - step) % size * rows, 0)
    return whole


def by_rep(block):
    return [block] + [shifted(block, "rep", step) for step in range(1, lax.axis_size("rep"))]


def group_rows(share_block):
    return jnp.concatenate([spread(block, "tp") for block in by_rep(share_block)])


def reduce_rows(partial, share):
    n_tp, tp, n_rep = (lax.axis_size("tp"), lax.axis_index("tp"), lax.axis_size("rep"))
    groups = partial.reshape(n_rep, n_tp, share, partial.shape[1])

    def chunk(step):
        return lax.dynamic_index_in_dim(groups, (tp + step) % n_tp, 1, keepdims=False)

    total = chunk(0).astype(jnp.float32)
    for step in range(1, n_tp):
        total = total + shifted(chunk(step), "tp", step).astype(jnp.float32)
    own = total[0]
    for step in range(1, n_rep):
        own = own + shifted(total[step].astype(jnp.bfloat16), "rep", -step).astype(jnp.float32)
    return own


def local(
    tokens,
    mix_gain,
    value_weight,
    outer_gate_weight,
    inner_gate_weight,
    conv_taps,
    mix_out_weight,
    ffn_gain,
    gate_weight,
    up_weight,
    down_weight,
):
    row_count = tokens.shape[0]
    share = row_count // lax.axis_size("tp")
    seq_len = row_count // SEQ_GRP
    n_rep, rep = (lax.axis_size("rep"), lax.axis_index("rep"))

    def part(array, axis):
        size = array.shape[axis] // n_rep
        return lax.dynamic_slice_in_dim(array, rep * size, size, axis)

    own_tokens = lax.dynamic_slice_in_dim(tokens, lax.axis_index("tp") * share, share, 0)
    conv_in = jnp.concatenate(
        [part(w, 1) for w in (value_weight, outer_gate_weight, inner_gate_weight)], axis=1
    )
    conv_full = lax.all_gather(conv_in, "fs", axis=0, tiled=True)
    mix_out_full = lax.all_gather(part(mix_out_weight, 0), "fs", axis=1, tiled=True)
    ffn_in = jnp.concatenate([part(w, 1) for w in (gate_weight, up_weight)], axis=1)
    ffn_full = lax.all_gather(ffn_in, "fs", axis=0, tiled=True)
    down_full = lax.all_gather(part(down_weight, 0), "fs", axis=1, tiled=True)
    normed = rms_norm(tokens, mix_gain)
    own_normed = lax.dynamic_slice_in_dim(normed, lax.axis_index("tp") * share, share, 0)
    rows = jnp.concatenate([normed] + [spread(b, "tp") for b in by_rep(own_normed)[1:]])
    proj = jnp.dot(rows, conv_full, preferred_element_type=jnp.float32).astype(jnp.bfloat16)
    value_proj, outer_proj, inner_proj = jnp.split(proj, 3, axis=1)
    mixed = short_conv(value_proj, outer_proj, inner_proj, part(conv_taps, 1), seq_len)
    mix_total = reduce_rows(
        jnp.dot(mixed, mix_out_full, preferred_element_type=jnp.float32).astype(jnp.bfloat16), share
    )
    after_mix = (own_tokens.astype(jnp.float32) + mix_total).astype(jnp.bfloat16)
    block_rows = group_rows(rms_norm(after_mix, ffn_gain))
    both = jnp.dot(block_rows, ffn_full, preferred_element_type=jnp.float32)
    gate_proj, up_proj = jnp.split(both, 2, axis=1)
    hidden = (jax.nn.silu(gate_proj) * up_proj).astype(jnp.bfloat16)
    ffn_total = reduce_rows(
        jnp.dot(hidden, down_full, preferred_element_type=jnp.float32).astype(jnp.bfloat16), share
    )
    finished = (after_mix.astype(jnp.float32) + ffn_total).astype(jnp.bfloat16)
    return spread(finished, "tp")


def solution(mesh):
    placed = (
        P(("rep", "fs"), None),
        P(),
        P("fs", "tp"),
        P("fs", "tp"),
        P("fs", "tp"),
        P(None, "tp"),
        P("tp", "fs"),
        P(),
        P("fs", "tp"),
        P("fs", "tp"),
        P("tp", "fs"),
    )
    return jax.shard_map(
        local, mesh=mesh, in_specs=placed, out_specs=P(("rep", "fs"), None), check_vma=False
    )
```

profile of v0, /device:TPU:0, one launch (start us, length us, event | category | flops | bytes accessed | tf_op | source)
XLA Modules:
  0.0 387.4 jit_solution(13555058826445362777)
XLA Ops:
  15.6 3.0 collective-permute-start
  18.6 23.3 %collective-permute-done = bf16[256,2048]{1,0:T(8,128)(2,1)} collective-permute-done((bf16[256,2048]{1,0:T(8,128)(2,1)S(1)}, bf16[256,2048]{1,0:T(8,128)(2,1)}, u32[]{:S(2)}, u32[]{:S(2)}) %collective-permute-start) | collective-permute-done | bytes 1048608 | tf_op jit(solution)/shard_map/ppermute | solution.py:32
  41.9 2.9 collective-permute-done.1
  44.9 3.0 broadcast_select_fusion.7
  47.9 43.9 %all-gather.5.cloned.1.call-done = bf16[2048,1152]{1,0:T(8,128)(2,1)} async-done(((bf16[256,1152]{1,0:T(8,128)(2,1)}), bf16[2048,1152]{1,0:T(8,128)(2,1)}) %all-gather.5.cloned.1.call-update) | async-done | bytes 4718608 | tf_op jit(solution)/shard_map/all_gather | solution.py:98
  91.8 9.8 %fusion.18 = bf16[1024,1152]{1,0:T(8,128)(2,1)S(1)} fusion(bf16[2048,1152]{1,0:T(8,128)(2,1)} %all-gather.5.cloned.1.call-done, bf16[256,2048]{1,0:T(8,128)(2,1)} %get-tuple-element.17, bf16[256,2048]{1,0:T(8,128)(2,1)} %get-tuple-element.16, bf16[512,2048]{1,0:T(8,128)(2,1)} %copy-done.3), kind=kOutput, calls=%fused_computation.24 | convolution fusion | flops 4845600768 | bytes 11272192 | tf_op jit(solution)/shard_map/dot_general | solution.py:106
  104.4 32.2 %all-gather.7.cloned.1.call-done = bf16[384,2048]{1,0:T(8,128)(2,1)} async-done(((bf16[384,256]{1,0:T(8,128)(2,1)}), bf16[384,2048]{1,0:T(8,128)(2,1)}) %all-gather.7.cloned.1.call-update) | async-done | bytes 1572880 | tf_op jit(solution)/shard_map/all_gather | solution.py:99
  136.6 6.0 %convolution_convert_fusion = bf16[1024,2048]{1,0:T(8,128)(2,1)S(1)} fusion(bf16[384,2048]{1,0:T(8,128)(2,1)} %all-gather.7.cloned.1.call-done, f32[1023,384]{1,0:T(8,128)} %bitcast.45, f32[1022,384]{1,0:T(8,128)} %bitcast.46, bf16[1024,1152]{1,0:T(8,128)(2,1)} %copy-done.5, f32[384]{0:T(512)S(1)} %get-tuple-element.6, f32[384]{0:T(512)S(1)} %get-tuple-element.7, ...), kind=kOutput, calls=%fused_computation.23 | convolution fusion | flops 1617821696 | bytes 11274240 | tf_op jit(solution)/shard_map/dot_general | solution.py:110
  142.7 2.0 copy-done.4
  144.7 1.6 dynamic-slice_bitcast_fusion.1
  147.1 3.6 collective-permute-done.2
  150.7 3.0 convert_add_fusion.1
  155.5 23.7 %collective-permute-done.3 = bf16[256,2048]{1,0:T(8,128)(2,1)S(1)} collective-permute-done((bf16[256,2048]{1,0:T(8,128)(2,1)S(1)}, bf16[256,2048]{1,0:T(8,128)(2,1)S(1)}, u32[]{:S(2)}, u32[]{:S(2)}) %collective-permute-start.3) | collective-permute-done | bytes 1048608 | tf_op jit(solution)/shard_map/ppermute | solution.py:32
  181.7 23.0 %collective-permute-done.5 = bf16[256,2048]{1,0:T(8,128)(2,1)S(1)} collective-permute-done((bf16[256,2048]{1,0:T(8,128)(2,1)S(1)}, bf16[256,2048]{1,0:T(8,128)(2,1)S(1)}, u32[]{:S(2)}, u32[]{:S(2)}) %collective-permute-start.5) | collective-permute-done | bytes 1048608 | tf_op jit(solution)/shard_map/ppermute | solution.py:32
  205.4 1.9 collective-permute-done.6
  208.8 52.6 %all-gather.9.cloned.1.call-done = bf16[2048,2048]{1,0:T(8,128)(2,1)} async-done(((bf16[256,2048]{1,0:T(8,128)(2,1)}), bf16[2048,2048]{1,0:T(8,128)(2,1)}) %all-gather.9.cloned.1.call-update) | async-done | bytes 8388624 | tf_op jit(solution)/shard_map/all_gather | solution.py:101
  261.5 13.8 %fusion.10 = f32[1024,2048]{1,0:T(8,128)} fusion(bf16[2048,2048]{1,0:T(8,128)(2,1)} %all-gather.9.cloned.1.call-done, bf16[256,2048]{1,0:T(8,128)(2,1)} %get-tuple-element.15, bf16[256,2048]{1,0:T(8,128)(2,1)} %get-tuple-element.14, bf16[256,2048]{1,0:T(8,128)(2,1)S(1)} %get-tuple-element.13, bf16[256,2048]{1,0:T(8,128)(2,1)S(1)} %get-tuple-element.12), kind=kOutput, calls=%fused_computation.13 | convolution fusion | flops 8606711808 | bytes 20971520 | tf_op jit(solution)/shard_map/dot_general | solution.py:114
  275.3 60.9 %all-gather.11.cloned.1.call-done = bf16[1024,2048]{1,0:T(8,128)(2,1)} async-done(((bf16[1024,256]{1,0:T(8,128)(2,1)}), bf16[1024,2048]{1,0:T(8,128)(2,1)}) %all-gather.11.cloned.1.call-update) | async-done | bytes 4194320 | tf_op jit(solution)/shard_map/all_gather | solution.py:102
  336.2 9.2 %convolution_convert_fusion.1 = bf16[1024,2048]{1,0:T(8,128)(2,1)S(1)} fusion(bf16[1024,2048]{1,0:T(8,128)(2,1)} %all-gather.11.cloned.1.call-done, f32[1024,2048]{1,0:T(8,128)} %fusion.10), kind=kOutput, calls=%fused_computation.25 | convolution fusion | flops 4303355904 | bytes 16777216 | tf_op jit(solution)/shard_map/dot_general | solution.py:118
  345.6 4.1 %collective-permute-done.7 = bf16[2,256,2048]{2,1,0:T(8,128)(2,1)S(1)} collective-permute-done((bf16[2,256,2048]{2,1,0:T(8,128)(2,1)S(1)}, bf16[2,256,2048]{2,1,0:T(8,128)(2,1)S(1)}, u32[]{:S(2)}, u32[]{:S(2)}) %collective-permute-start.7) | collective-permute-done | bytes 2097184 | tf_op jit(solution)/shard_map/ppermute | solution.py:32
  350.7 1.6 collective-permute-start.8
  352.3 23.7 %collective-permute-done.8 = bf16[256,2048]{1,0:T(8,128)(2,1)S(1)} collective-permute-done((bf16[256,2048]{1,0:T(8,128)(2,1)S(1)}, bf16[256,2048]{1,0:T(8,128)(2,1)S(1)}, u32[]{:S(2)}, u32[]{:S(2)}) %collective-permute-start.8) | collective-permute-done | bytes 1048608 | tf_op jit(solution)/shard_map/ppermute | solution.py:32
  376.5 2.6 collective-permute-done.9
  379.3 1.6 pad_maximum_fusion
  (64 shorter events, 20.7 us)
Async XLA Ops:
  6.5 139.7 %copy-start = (bf16[2048,256]{1,0:T(8,128)(2,1)S(1)}, bf16[2048,256]{1,0:T(8,128)(2,1)}, u32[]{:S(2)}) copy-start(bf16[2048,256]{1,0:T(8,128)(2,1)} %param.21) | copy-start | bytes 3145732
  6.5 3.1 copy-start.6
  6.5 85.3 %all-gather.5.cloned.1.call-start = ((), (), s32[]{:S(2)}) async-start(), calls=%async_computation | async-start | bytes 5308416 | tf_op jit(solution)/shard_map/all_gather | solution.py:98
  9.6 127.1 %all-gather.7.cloned.1.call-start = ((), (), s32[]{:S(2)}) async-start(), calls=%async_computation.1 | async-start | bytes 1769472 | tf_op jit(solution)/shard_map/all_gather | solution.py:99
  10.4 251.1 %all-gather.9.cloned.1.call-start = ((), (), s32[]{:S(2)}) async-start(), calls=%async_computation.2 | async-start | bytes 9437184 | tf_op jit(solution)/shard_map/all_gather | solution.py:101
  10.4 2.6 copy-start.7
  10.4 2.6 copy-start.2
  13.0 323.2 %all-gather.11.cloned.1.call-start = ((), (), s32[]{:S(2)}) async-start(), calls=%async_computation.3 | async-start | bytes 4718592 | tf_op jit(solution)/shard_map/all_gather | solution.py:102
  13.6 28.3 %copy-start.9 = (bf16[3,768]{1,0:T(4,128)(2,1)S(1)}, bf16[3,768]{1,0:T(4,128)(2,1)}, u32[]{:S(2)}) copy-start(bf16[3,768]{1,0:T(4,128)(2,1)} %param.16) | copy-start | bytes 13828
  14.1 1.3 copy-start.3
  15.6 26.3 %collective-permute-start = (bf16[256,2048]{1,0:T(8,128)(2,1)S(1)}, bf16[256,2048]{1,0:T(8,128)(2,1)}, u32[]{:S(2)}, u32[]{:S(2)}) collective-permute-start(bf16[256,2048]{1,0:T(8,128)(2,1)S(1)} %constant_dynamic-slice_fusion.8), channel_id=1, source_target_pairs={{0,16},{16,0},{1,17},{17,1},{2,18},{18,2},{3,19},{19,3},{4,20},{20... | collective-permute-start | bytes 3145736 | tf_op jit(solution)/shard_map/ppermute | solution.py:32
  41.9 3.0 collective-permute-start.1
  101.6 1.5 copy-start.5
  142.7 2.0 copy-start.4
  146.2 4.5 %collective-permute-start.2 = (bf16[2,256,2048]{2,1,0:T(8,128)(2,1)}, bf16[2,256,2048]{2,1,0:T(8,128)(2,1)}, u32[]{:S(2)}, u32[]{:S(2)}) collective-permute-start(bf16[2,256,2048]{2,1,0:T(8,128)(2,1)} %dynamic-slice_bitcast_fusion.1), channel_id=1, source_target_pairs={{0,1},{1,0},{2,3},{3,2},{4,5},{5,4},{6,7},{7,6},{8,9},{9,8},{10,11... | collective-permute-start | bytes 6291464 | tf_op jit(solution)/shard_map/ppermute | solution.py:32
  147.1 8.4 %copy-start.8 = (bf16[2048]{0:T(1024)(128)(2,1)S(1)}, bf16[2048]{0:T(1024)(128)(2,1)}, u32[]{:S(2)}) copy-start(bf16[2048]{0:T(1024)(128)(2,1)} %param.18) | copy-start | bytes 12292
  153.9 25.3 %collective-permute-start.3 = (bf16[256,2048]{1,0:T(8,128)(2,1)S(1)}, bf16[256,2048]{1,0:T(8,128)(2,1)S(1)}, u32[]{:S(2)}, u32[]{:S(2)}) collective-permute-start(bf16[256,2048]{1,0:T(8,128)(2,1)S(1)} %fusion.31), channel_id=1, source_target_pairs={{0,16},{16,0},{1,17},{17,1},{2,18},{18,2},{3,19},{19,3},{4,20},{20... | collective-permute-start | bytes 3145736 | tf_op jit(solution)/shard_map/ppermute | solution.py:32
  180.2 24.5 %collective-permute-start.5 = (bf16[256,2048]{1,0:T(8,128)(2,1)S(1)}, bf16[256,2048]{1,0:T(8,128)(2,1)S(1)}, u32[]{:S(2)}, u32[]{:S(2)}) collective-permute-start(bf16[256,2048]{1,0:T(8,128)(2,1)S(1)} %fusion.23), channel_id=1, source_target_pairs={{0,16},{16,0},{1,17},{17,1},{2,18},{18,2},{3,19},{19,3},{4,20},{20... | collective-permute-start | bytes 3145736 | tf_op jit(solution)/shard_map/ppermute | solution.py:32
  181.7 23.0 %collective-permute-start.4 = (bf16[256,2048]{1,0:T(8,128)(2,1)S(1)}, bf16[256,2048]{1,0:T(8,128)(2,1)S(1)}, u32[]{:S(2)}, u32[]{:S(2)}) collective-permute-start(bf16[256,2048]{1,0:T(8,128)(2,1)S(1)} %fusion.23), channel_id=1, source_target_pairs={{0,1},{1,0},{2,3},{3,2},{4,5},{5,4},{6,7},{7,6},{8,9},{9,8},{10,11... | collective-permute-start | bytes 3145736 | tf_op jit(solution)/shard_map/ppermute | solution.py:32
  204.7 2.7 collective-permute-start.6
  345.6 4.2 %collective-permute-start.7 = (bf16[2,256,2048]{2,1,0:T(8,128)(2,1)S(1)}, bf16[2,256,2048]{2,1,0:T(8,128)(2,1)S(1)}, u32[]{:S(2)}, u32[]{:S(2)}) collective-permute-start(bf16[2,256,2048]{2,1,0:T(8,128)(2,1)S(1)} %dynamic-slice_bitcast_fusion), channel_id=1, source_target_pairs={{0,1},{1,0},{2,3},{3,2},{4,5},{5,4},{6,7},{7,6},{8,9},{9,8},{10,11... | collective-permute-start | bytes 6291464 | tf_op jit(solution)/shard_map/ppermute | solution.py:32
  350.7 25.3 %collective-permute-start.8 = (bf16[256,2048]{1,0:T(8,128)(2,1)S(1)}, bf16[256,2048]{1,0:T(8,128)(2,1)S(1)}, u32[]{:S(2)}, u32[]{:S(2)}) collective-permute-start(bf16[256,2048]{1,0:T(8,128)(2,1)S(1)} %fusion.32), channel_id=1, source_target_pairs={{0,16},{16,0},{1,17},{17,1},{2,18},{18,2},{3,19},{19,3},{4,20},{20... | collective-permute-start | bytes 3145736 | tf_op jit(solution)/shard_map/ppermute | solution.py:32
  376.5 2.7 collective-permute-start.9
  379.2 1.7 copy-start.1
Sparse Core Ops, SparseCore 0:
  9.7 82.0 all-gather.4
  93.8 42.7 all-gather.6
  138.8 122.6 all-gather.8
  263.4 72.8 all-gather.10
where the time goes:
time: 388 us; the launch traced here: 387 us
  waiting for transfers between devices  299 us (77%)
  matrix products  38.9 us (10%)
  other arithmetic  16.5 us (4%)
  between operations  13.4 us (3%)
  local copies, waits for them, and re-layouts  12 us (3%)
  starting transfers between devices  7.97 us (2%)
    ppermute x10, waiting for transfers between devices, shifted(): lax.ppermute(values, axis, [(i, (i + step) % size) for i in range(size)])  109 us
    all_gather x1, waiting for transfers between devices, local(): down_full = lax.all_gather(part(down_weight, 0), 'fs', axis=1, tiled=True)  60.9 us
    all_gather x1, waiting for transfers between devices, local(): ffn_full = lax.all_gather(ffn_in, 'fs', axis=0, tiled=True)  52.6 us
    all_gather x1, waiting for transfers between devices, local(): conv_full = lax.all_gather(conv_in, 'fs', axis=0, tiled=True)  43.9 us
    all_gather x1, waiting for transfers between devices, local(): lax.all_gather(part(mix_out_weight, 0), 'fs', axis=1, tiled=True)  32.2 us
    dot_general x1, matrix products, local(): both = jnp.dot(block_rows, ffn_full, preferred_element_type=jnp.float32)  13.8 us
    dot_general x1, matrix products, local(): jnp.dot(rows, conv_full, preferred_element_type=jnp.float32)  9.83 us
    dot_general x1, matrix products, local(): jnp.dot(hidden, down_full, preferred_element_type=jnp.float32)  9.19 us
  transfers between devices with their start and end apart: 14, of which 13 were waited for; matrix products, arithmetic and copies ran while one was open for 12% of the time, Pallas kernels for 0%

commit v1 on v0

--- a/solution.py
+++ b/solution.py
@@ -95,7 +95,12 @@
     conv_in = jnp.concatenate(
         [part(w, 1) for w in (value_weight, outer_gate_weight, inner_gate_weight)], axis=1
     )
-    conv_full = lax.all_gather(conv_in, "fs", axis=0, tiled=True)
+    ring = [conv_in]
+    for hop in range(7):
+        ring.append(lax.ppermute(ring[-1], "fs", [(dev, (dev + 1) % 8) for dev in range(8)]))
+    conv_full = jnp.roll(
+        jnp.concatenate(ring[::-1], axis=0), (lax.axis_index("fs") + 1) * ring[0].shape[0], axis=0
+    )
     mix_out_full = lax.all_gather(part(mix_out_weight, 0), "fs", axis=1, tiled=True)
     ffn_in = jnp.concatenate([part(w, 1) for w in (gate_weight, up_weight)], axis=1)
     ffn_full = lax.all_gather(ffn_in, "fs", axis=0, tiled=True)

time: 388 us -> 363 us (0.936)
  waiting for transfers between devices: 299 us -> 269 us
  local copies, waits for them, and re-layouts: 12 us -> 20.3 us
    ppermute x0 -> x7, waiting for transfers between devices: none -> 160 us  [local(): lax.ppermute(ring[-1], 'fs', [(dev, (dev + 1) % 8) for dev in range(8)])]
    all_gather x1, waiting for transfers between devices: 52.6 us -> 0.01 us  [local(): ffn_full = lax.all_gather(ffn_in, 'fs', axis=0, tiled=True)]
    all_gather x1 -> x0, waiting for transfers between devices: 43.9 us -> none  [local(): conv_full = lax.all_gather(conv_in, 'fs', axis=0, tiled=True)]
    all_gather x1, waiting for transfers between devices: 60.9 us -> 25 us  [local(): down_full = lax.all_gather(part(down_weight, 0), 'fs', axis=1, tiled=True)]
    all_gather x1, waiting for transfers between devices: 32.2 us -> 0.02 us  [local(): lax.all_gather(part(mix_out_weight, 0), 'fs', axis=1, tiled=True)]
    ppermute x10, waiting for transfers between devices: 109 us -> 83.9 us  [shifted(): lax.ppermute(values, axis, [(i, (i + step) % size) for i in range(size)])]
    unnamed x20 -> x42, local copies, waits for them, and re-layouts: 4.81 us -> 12.5 us
  transfers between devices with their start and end apart: 14 -> 20, of which waited for: 13 -> 15; matrix products, arithmetic and copies ran while one was open for 12% -> 14% of each run, Pallas kernels for 0% -> 0%
where the time goes in v1:
time: 363 us; the launch traced here: 362 us
  waiting for transfers between devices  269 us (74%)
  matrix products  36.6 us (10%)
  local copies, waits for them, and re-layouts  20.3 us (6%)
  other arithmetic  14.7 us (4%)
  between operations  13.6 us (4%)
  starting transfers between devices  7.89 us (2%)
    ppermute x7, waiting for transfers between devices, local(): lax.ppermute(ring[-1], 'fs', [(dev, (dev + 1) % 8) for dev in range(8)])  160 us
    ppermute x10, waiting for transfers between devices, shifted(): lax.ppermute(values, axis, [(i, (i + step) % size) for i in range(size)])  83.9 us
    all_gather x1, waiting for transfers between devices, local(): down_full = lax.all_gather(part(down_weight, 0), 'fs', axis=1, tiled=True)  25 us
    dot_general x1, matrix products, local(): both = jnp.dot(block_rows, ffn_full, preferred_element_type=jnp.float32)  14.1 us
    unnamed x42, local copies, waits for them, and re-layouts  12.5 us
    dot_general x1, matrix products, local(): jnp.dot(hidden, down_full, preferred_element_type=jnp.float32)  9.19 us
    dot_general x1, matrix products, local(): jnp.dot(rows, conv_full, preferred_element_type=jnp.float32)  8.16 us
  transfers between devices with their start and end apart: 20, of which 15 were waited for; matrix products, arithmetic and copies ran while one was open for 14% of the time, Pallas kernels for 0%

profile of v1, /device:TPU:0, one launch (start us, length us, event | category | flops | bytes accessed | tf_op | source)
XLA Modules:
  0.0 362.1 jit_solution(5485506010560912385)
XLA Ops:
  6.6 1.8 constant_dynamic-slice_fusion.3
  13.6 3.0 collective-permute-start.2
  16.7 22.3 %collective-permute-done.2 = bf16[256,1152]{1,0:T(8,128)(2,1)S(1)} collective-permute-done((bf16[256,1152]{1,0:T(8,128)(2,1)S(1)}, bf16[256,1152]{1,0:T(8,128)(2,1)S(1)}, u32[]{:S(2)}, u32[]{:S(2)}) %collective-permute-start.2) | collective-permute-done | bytes 589856 | tf_op jit(solution)/shard_map/ppermute | solution.py:100
  40.4 25.9 %collective-permute-done.3 = bf16[256,1152]{1,0:T(8,128)(2,1)} collective-permute-done((bf16[256,1152]{1,0:T(8,128)(2,1)S(1)}, bf16[256,1152]{1,0:T(8,128)(2,1)}, u32[]{:S(2)}, u32[]{:S(2)}) %collective-permute-start.3) | collective-permute-done | bytes 589856 | tf_op jit(solution)/shard_map/ppermute | solution.py:100
  66.3 1.9 fusion.4
  70.9 10.1 %collective-permute-done.4 = bf16[256,1152]{1,0:T(8,128)(2,1)} collective-permute-done((bf16[256,1152]{1,0:T(8,128)(2,1)}, bf16[256,1152]{1,0:T(8,128)(2,1)}, u32[]{:S(2)}, u32[]{:S(2)}) %collective-permute-start.4) | collective-permute-done | bytes 589856 | tf_op jit(solution)/shard_map/ppermute | solution.py:100
  81.0 29.9 %collective-permute-done.5 = bf16[256,1152]{1,0:T(8,128)(2,1)S(1)} collective-permute-done((bf16[256,1152]{1,0:T(8,128)(2,1)}, bf16[256,1152]{1,0:T(8,128)(2,1)S(1)}, u32[]{:S(2)}, u32[]{:S(2)}) %collective-permute-start.5) | collective-permute-done | bytes 589856 | tf_op jit(solution)/shard_map/ppermute | solution.py:100
  111.0 29.7 %collective-permute-done.6 = bf16[256,1152]{1,0:T(8,128)(2,1)S(1)} collective-permute-done((bf16[256,1152]{1,0:T(8,128)(2,1)S(1)}, bf16[256,1152]{1,0:T(8,128)(2,1)S(1)}, u32[]{:S(2)}, u32[]{:S(2)}) %collective-permute-start.6) | collective-permute-done | bytes 589856 | tf_op jit(solution)/shard_map/ppermute | solution.py:100
  140.7 14.9 %collective-permute-done.7 = bf16[256,1152]{1,0:T(8,128)(2,1)S(1)} collective-permute-done((bf16[256,1152]{1,0:T(8,128)(2,1)S(1)}, bf16[256,1152]{1,0:T(8,128)(2,1)S(1)}, u32[]{:S(2)}, u32[]{:S(2)}) %collective-permute-start.7) | collective-permute-done | bytes 589856 | tf_op jit(solution)/shard_map/ppermute | solution.py:100
  157.4 27.2 %collective-permute-done.8 = bf16[256,1152]{1,0:T(8,128)(2,1)} collective-permute-done((bf16[256,1152]{1,0:T(8,128)(2,1)S(1)}, bf16[256,1152]{1,0:T(8,128)(2,1)}, u32[]{:S(2)}, u32[]{:S(2)}) %collective-permute-start.8) | collective-permute-done | bytes 589856 | tf_op jit(solution)/shard_map/ppermute | solution.py:100
  192.4 8.2 %fusion.19 = bf16[1024,1152]{1,0:T(8,128)(2,1)S(1)} fusion(bf16[4096,1152]{1,0:T(8,128)(2,1)S(1)} %constant_dynamic-update-slice_fusion, s32[]{:T(128)S(6)} %select_n.116, bf16[256,2048]{1,0:T(8,128)(2,1)S(1)} %get-tuple-element.17, bf16[256,2048]{1,0:T(8,128)(2,1)S(1)} %get-tuple-element.16, bf16[512,2048]{1,0:T(8,128)(2,1)S(1)} %copy-done.4), kind=kOutput, calls=%fused_computation.25 | convolution fusion | flops 4845600768 | bytes 11272196 | tf_op jit(solution)/shard_map/dot_general | solution.py:111
  202.2 5.1 %convolution_convert_fusion = bf16[1024,2048]{1,0:T(8,128)(2,1)S(1)} fusion(bf16[384,2048]{1,0:T(8,128)(2,1)} %all-gather.4.cloned.1.call-done, f32[1023,384]{1,0:T(8,128)S(1)} %bitcast.44, f32[1022,384]{1,0:T(8,128)S(1)} %bitcast.45, bf16[1024,1152]{1,0:T(8,128)(2,1)} %copy-done.10, f32[384]{0:T(512)S(1)} %get-tuple-element.6, ...), kind=kOutput, calls=%fused_computation.24 | convolution fusion | flops 1617821696 | bytes 11274240 | tf_op jit(solution)/shard_map/dot_general | solution.py:115
  207.3 2.0 copy-done.5
  210.5 3.4 collective-permute-done.9
  213.8 3.0 convert_add_fusion.1
  217.8 24.5 %collective-permute-done.10 = bf16[256,2048]{1,0:T(8,128)(2,1)S(1)} collective-permute-done((bf16[256,2048]{1,0:T(8,128)(2,1)S(1)}, bf16[256,2048]{1,0:T(8,128)(2,1)S(1)}, u32[]{:S(2)}, u32[]{:S(2)}) %collective-permute-start.10) | collective-permute-done | bytes 1048608 | tf_op jit(solution)/shard_map/ppermute | solution.py:32
  244.0 23.7 %collective-permute-done.12 = bf16[256,2048]{1,0:T(8,128)(2,1)S(1)} collective-permute-done((bf16[256,2048]{1,0:T(8,128)(2,1)S(1)}, bf16[256,2048]{1,0:T(8,128)(2,1)S(1)}, u32[]{:S(2)}, u32[]{:S(2)}) %collective-permute-start.12) | collective-permute-done | bytes 1048608 | tf_op jit(solution)/shard_map/ppermute | solution.py:32
  268.3 1.9 collective-permute-done.13
  271.8 14.1 %fusion.11 = f32[1024,2048]{1,0:T(8,128)} fusion(bf16[2048,2048]{1,0:T(8,128)(2,1)} %all-gather.6.cloned.1.call-done, bf16[256,2048]{1,0:T(8,128)(2,1)} %get-tuple-element.15, bf16[256,2048]{1,0:T(8,128)(2,1)} %get-tuple-element.14, bf16[256,2048]{1,0:T(8,128)(2,1)S(1)} %get-tuple-element.13, bf16[256,2048]{1,0:T(8,128)(2,1)S(1)} %get-tuple-element.12), kind=kOutput, calls=%fused_computation.14 | convolution fusion | flops 8606711808 | bytes 20971520 | tf_op jit(solution)/shard_map/dot_general | solution.py:119
  285.9 25.0 %all-gather.8.cloned.1.call-done = bf16[1024,2048]{1,0:T(8,128)(2,1)} async-done(((bf16[1024,256]{1,0:T(8,128)(2,1)}), bf16[1024,2048]{1,0:T(8,128)(2,1)}) %all-gather.8.cloned.1.call-update) | async-done | bytes 4194320 | tf_op jit(solution)/shard_map/all_gather | solution.py:107
  310.9 9.2 %convolution_convert_fusion.1 = bf16[1024,2048]{1,0:T(8,128)(2,1)S(1)} fusion(bf16[1024,2048]{1,0:T(8,128)(2,1)} %all-gather.8.cloned.1.call-done, f32[1024,2048]{1,0:T(8,128)} %fusion.11), kind=kOutput, calls=%fused_computation.26 | convolution fusion | flops 4303355904 | bytes 16777216 | tf_op jit(solution)/shard_map/dot_general | solution.py:123
  320.3 4.1 %collective-permute-done.14 = bf16[2,256,2048]{2,1,0:T(8,128)(2,1)S(1)} collective-permute-done((bf16[2,256,2048]{2,1,0:T(8,128)(2,1)S(1)}, bf16[2,256,2048]{2,1,0:T(8,128)(2,1)S(1)}, u32[]{:S(2)}, u32[]{:S(2)}) %collective-permute-start.14) | collective-permute-done | bytes 2097184 | tf_op jit(solution)/shard_map/ppermute | solution.py:32
  327.0 23.7 %collective-permute-done.15 = bf16[256,2048]{1,0:T(8,128)(2,1)S(1)} collective-permute-done((bf16[256,2048]{1,0:T(8,128)(2,1)S(1)}, bf16[256,2048]{1,0:T(8,128)(2,1)S(1)}, u32[]{:S(2)}, u32[]{:S(2)}) %collective-permute-start.15) | collective-permute-done | bytes 1048608 | tf_op jit(solution)/shard_map/ppermute | solution.py:32
  351.2 2.6 collective-permute-done.16
  (99 shorter events, 31.2 us)
Async XLA Ops:
  6.5 203.0 %copy-start = (bf16[2048,256]{1,0:T(8,128)(2,1)S(1)}, bf16[2048,256]{1,0:T(8,128)(2,1)}, u32[]{:S(2)}) copy-start(bf16[2048,256]{1,0:T(8,128)(2,1)} %param.21) | copy-start | bytes 3145732
  6.5 33.3 %copy-start.11 = (bf16[2048]{0:T(1024)(128)(2,1)S(1)}, bf16[2048]{0:T(1024)(128)(2,1)}, u32[]{:S(2)}) copy-start(bf16[2048]{0:T(1024)(128)(2,1)} %param.12) | copy-start | bytes 12292
  6.5 33.3 %copy-start.2 = (bf16[512,2048]{1,0:T(8,128)(2,1)S(1)}, bf16[512,2048]{1,0:T(8,128)(2,1)}, u32[]{:S(2)}) copy-start(bf16[512,2048]{1,0:T(8,128)(2,1)} %param.11) | copy-start | bytes 6291460
  6.5 195.6 %all-gather.4.cloned.1.call-start = ((), (), s32[]{:S(2)}) async-start(), calls=%async_computation | async-start | bytes 1769472 | tf_op jit(solution)/shard_map/all_gather | solution.py:104
  8.4 263.5 %all-gather.6.cloned.1.call-start = ((), (), s32[]{:S(2)}) async-start(), calls=%async_computation.1 | async-start | bytes 9437184 | tf_op jit(solution)/shard_map/all_gather | solution.py:106
  10.8 300.1 %all-gather.8.cloned.1.call-start = ((), (), s32[]{:S(2)}) async-start(), calls=%async_computation.2 | async-start | bytes 4718592 | tf_op jit(solution)/shard_map/all_gather | solution.py:107
  13.6 25.4 %collective-permute-start.2 = (bf16[256,1152]{1,0:T(8,128)(2,1)S(1)}, bf16[256,1152]{1,0:T(8,128)(2,1)S(1)}, u32[]{:S(2)}, u32[]{:S(2)}) collective-permute-start(bf16[256,1152]{1,0:T(8,128)(2,1)S(1)} %pad_maximum_fusion.2), channel_id=1, source_target_pairs={{0,2},{2,4},{4,6},{6,8},{8,10},{10,12},{12,14},{14,0},{1,3},{3,5},... | collective-permute-start | bytes 1769480 | tf_op jit(solution)/shard_map/ppermute | solution.py:100
  39.8 26.5 %collective-permute-start.3 = (bf16[256,1152]{1,0:T(8,128)(2,1)S(1)}, bf16[256,1152]{1,0:T(8,128)(2,1)}, u32[]{:S(2)}, u32[]{:S(2)}) collective-permute-start(bf16[256,1152]{1,0:T(8,128)(2,1)S(1)} %collective-permute-done.2), channel_id=1, source_target_pairs={{0,2},{2,4},{4,6},{6,8},{8,10},{10,12},{12,14},{14,0},{1,3},{3,5},... | collective-permute-start | bytes 1769480 | tf_op jit(solution)/shard_map/ppermute | solution.py:100
  39.9 100.9 %copy-start.13 = (bf16[3,768]{1,0:T(4,128)(2,1)S(1)}, bf16[3,768]{1,0:T(4,128)(2,1)}, u32[]{:S(2)}) copy-start(bf16[3,768]{1,0:T(4,128)(2,1)} %param.16) | copy-start | bytes 13828
  66.3 14.7 %collective-permute-start.4 = (bf16[256,1152]{1,0:T(8,128)(2,1)}, bf16[256,1152]{1,0:T(8,128)(2,1)}, u32[]{:S(2)}, u32[]{:S(2)}) collective-permute-start(bf16[256,1152]{1,0:T(8,128)(2,1)} %collective-permute-done.3), channel_id=1, source_target_pairs={{0,2},{2,4},{4,6},{6,8},{8,10},{10,12},{12,14},{14,0},{1,3},{3,5},... | collective-permute-start | bytes 1769480 | tf_op jit(solution)/shard_map/ppermute | solution.py:100
  69.5 41.5 %collective-permute-start = (bf16[256,2048]{1,0:T(8,128)(2,1)S(1)}, bf16[256,2048]{1,0:T(8,128)(2,1)}, u32[]{:S(2)}, u32[]{:S(2)}) collective-permute-start(bf16[256,2048]{1,0:T(8,128)(2,1)S(1)} %constant_dynamic-slice_fusion.8), channel_id=1, source_target_pairs={{0,16},{16,0},{1,17},{17,1},{2,18},{18,2},{3,19},{19,3},{4,20},{20... | collective-permute-start | bytes 3145736 | tf_op jit(solution)/shard_map/ppermute | solution.py:32
  81.0 29.9 %collective-permute-start.5 = (bf16[256,1152]{1,0:T(8,128)(2,1)}, bf16[256,1152]{1,0:T(8,128)(2,1)S(1)}, u32[]{:S(2)}, u32[]{:S(2)}) collective-permute-start(bf16[256,1152]{1,0:T(8,128)(2,1)} %collective-permute-done.4), channel_id=1, source_target_pairs={{0,2},{2,4},{4,6},{6,8},{8,10},{10,12},{12,14},{14,0},{1,3},{3,5},... | collective-permute-start | bytes 1769480 | tf_op jit(solution)/shard_map/ppermute | solution.py:100
  111.0 29.7 %collective-permute-start.6 = (bf16[256,1152]{1,0:T(8,128)(2,1)S(1)}, bf16[256,1152]{1,0:T(8,128)(2,1)S(1)}, u32[]{:S(2)}, u32[]{:S(2)}) collective-permute-start(bf16[256,1152]{1,0:T(8,128)(2,1)S(1)} %collective-permute-done.5), channel_id=1, source_target_pairs={{0,2},{2,4},{4,6},{6,8},{8,10},{10,12},{12,14},{14,0},{1,3},{3,5},... | collective-permute-start | bytes 1769480 | tf_op jit(solution)/shard_map/ppermute | solution.py:100
  111.0 44.7 %collective-permute-start.1 = (bf16[256,2048]{1,0:T(8,128)(2,1)}, bf16[256,2048]{1,0:T(8,128)(2,1)}, u32[]{:S(2)}, u32[]{:S(2)}) collective-permute-start(bf16[256,2048]{1,0:T(8,128)(2,1)} %collective-permute-done), channel_id=1, source_target_pairs={{0,1},{1,0},{2,3},{3,2},{4,5},{5,4},{6,7},{7,6},{8,9},{9,8},{10,11... | collective-permute-start | bytes 3145736 | tf_op jit(solution)/shard_map/ppermute | solution.py:32
  140.7 14.9 %collective-permute-start.7 = (bf16[256,1152]{1,0:T(8,128)(2,1)S(1)}, bf16[256,1152]{1,0:T(8,128)(2,1)S(1)}, u32[]{:S(2)}, u32[]{:S(2)}) collective-permute-start(bf16[256,1152]{1,0:T(8,128)(2,1)S(1)} %collective-permute-done.6), channel_id=1, source_target_pairs={{0,2},{2,4},{4,6},{6,8},{8,10},{10,12},{12,14},{14,0},{1,3},{3,5},... | collective-permute-start | bytes 1769480 | tf_op jit(solution)/shard_map/ppermute | solution.py:100
  155.6 29.0 %collective-permute-start.8 = (bf16[256,1152]{1,0:T(8,128)(2,1)S(1)}, bf16[256,1152]{1,0:T(8,128)(2,1)}, u32[]{:S(2)}, u32[]{:S(2)}) collective-permute-start(bf16[256,1152]{1,0:T(8,128)(2,1)S(1)} %collective-permute-done.7), channel_id=1, source_target_pairs={{0,2},{2,4},{4,6},{6,8},{8,10},{10,12},{12,14},{14,0},{1,3},{3,5},... | collective-permute-start | bytes 1769480 | tf_op jit(solution)/shard_map/ppermute | solution.py:100
  209.5 4.4 %collective-permute-start.9 = (bf16[2,256,2048]{2,1,0:T(8,128)(2,1)S(1)}, bf16[2,256,2048]{2,1,0:T(8,128)(2,1)}, u32[]{:S(2)}, u32[]{:S(2)}) collective-permute-start(bf16[2,256,2048]{2,1,0:T(8,128)(2,1)S(1)} %dynamic-slice_bitcast_fusion.1), channel_id=1, source_target_pairs={{0,1},{1,0},{2,3},{3,2},{4,5},{5,4},{6,7},{7,6},{8,9},{9,8},{10,11... | collective-permute-start | bytes 6291464 | tf_op jit(solution)/shard_map/ppermute | solution.py:32
  217.0 25.3 %collective-permute-start.10 = (bf16[256,2048]{1,0:T(8,128)(2,1)S(1)}, bf16[256,2048]{1,0:T(8,128)(2,1)S(1)}, u32[]{:S(2)}, u32[]{:S(2)}) collective-permute-start(bf16[256,2048]{1,0:T(8,128)(2,1)S(1)} %fusion.34), channel_id=1, source_target_pairs={{0,16},{16,0},{1,17},{17,1},{2,18},{18,2},{3,19},{19,3},{4,20},{20... | collective-permute-start | bytes 3145736 | tf_op jit(solution)/shard_map/ppermute | solution.py:32
  243.2 24.4 %collective-permute-start.12 = (bf16[256,2048]{1,0:T(8,128)(2,1)S(1)}, bf16[256,2048]{1,0:T(8,128)(2,1)S(1)}, u32[]{:S(2)}, u32[]{:S(2)}) collective-permute-start(bf16[256,2048]{1,0:T(8,128)(2,1)S(1)} %fusion.26), channel_id=1, source_target_pairs={{0,16},{16,0},{1,17},{17,1},{2,18},{18,2},{3,19},{19,3},{4,20},{20... | collective-permute-start | bytes 3145736 | tf_op jit(solution)/shard_map/ppermute | solution.py:32
  243.9 23.7 %collective-permute-start.11 = (bf16[256,2048]{1,0:T(8,128)(2,1)S(1)}, bf16[256,2048]{1,0:T(8,128)(2,1)S(1)}, u32[]{:S(2)}, u32[]{:S(2)}) collective-permute-start(bf16[256,2048]{1,0:T(8,128)(2,1)S(1)} %fusion.26), channel_id=1, source_target_pairs={{0,1},{1,0},{2,3},{3,2},{4,5},{5,4},{6,7},{7,6},{8,9},{9,8},{10,11... | collective-permute-start | bytes 3145736 | tf_op jit(solution)/shard_map/ppermute | solution.py:32
  267.6 2.7 collective-permute-start.13
  320.2 4.2 %collective-permute-start.14 = (bf16[2,256,2048]{2,1,0:T(8,128)(2,1)S(1)}, bf16[2,256,2048]{2,1,0:T(8,128)(2,1)S(1)}, u32[]{:S(2)}, u32[]{:S(2)}) collective-permute-start(bf16[2,256,2048]{2,1,0:T(8,128)(2,1)S(1)} %dynamic-slice_bitcast_fusion), channel_id=1, source_target_pairs={{0,1},{1,0},{2,3},{3,2},{4,5},{5,4},{6,7},{7,6},{8,9},{9,8},{10,11... | collective-permute-start | bytes 6291464 | tf_op jit(solution)/shard_map/ppermute | solution.py:32
  325.4 25.3 %collective-permute-start.15 = (bf16[256,2048]{1,0:T(8,128)(2,1)S(1)}, bf16[256,2048]{1,0:T(8,128)(2,1)S(1)}, u32[]{:S(2)}, u32[]{:S(2)}) collective-permute-start(bf16[256,2048]{1,0:T(8,128)(2,1)S(1)} %fusion.35), channel_id=1, source_target_pairs={{0,16},{16,0},{1,17},{17,1},{2,18},{18,2},{3,19},{19,3},{4,20},{20... | collective-permute-start | bytes 3145736 | tf_op jit(solution)/shard_map/ppermute | solution.py:32
  351.1 2.7 collective-permute-start.16
  (10 other events, 113.7 us)
Sparse Core Ops, SparseCore 0:
  9.4 59.2 all-gather.3
  70.8 164.1 all-gather.5
  237.1 73.7 all-gather.7
